TPU v7x, 32 devices: a whole 2x2x4 slice. The times are simulated.
32 devices in a mesh: grp: 2 (over y), sp: 4 (over z), tp: 4 (over x, core).
Axes of the slice: x: 2, y: 2, z: 4, core: 2. Of those that a mesh axis runs over, the one named last changes fastest.
Arguments:
- query_rows: bfloat16 [1024, 1024], P(('grp', 'sp'), 'tp'), parts along dimension 0, may hold values from -64 to 64
- key_rows: bfloat16 [1024, 512], P(('grp', 'sp'), 'tp'), parts along dimension 0, may hold values from -16 to 16
- value_rows: bfloat16 [1024, 512], P(('grp', 'sp'), 'tp'), parts along dimension 0, may hold values from -6 to 6
- sink_logit: float32 [16], P('tp'), may hold values from 3.5 to 7
- out_weight: bfloat16 [1024, 2048], P('tp'), may hold values from -0.1875 to 0.1875
- residual: bfloat16 [1024, 2048], P(('grp', 'sp', 'tp')), parts along dimension 0, may hold values from -6 to 6
- norm_gain: float32 [2048], replicated, may hold values from 0.1 to 1.9
- routes: int32 [1024, 6], P(('grp', 'sp', 'tp')), parts along dimension 0, may hold values from 0 to 15, as said below
- gate_weights: float32 [1024, 6], P(('grp', 'sp', 'tp')), parts along dimension 0, may hold values from 0.1 to 0.8
- expert_gate: bfloat16 [16, 2048, 512], P(('sp', 'tp')), may hold values from -0.125 to 0.125
- expert_up: bfloat16 [16, 2048, 512], P(('sp', 'tp')), may hold values from -0.125 to 0.125
- expert_down: bfloat16 [16, 512, 2048], P(('sp', 'tp')), may hold values from -0.25 to 0.25
- shared_gate: bfloat16 [2048, 512], P(None, 'tp'), may hold values from -0.125 to 0.125
- shared_up: bfloat16 [2048, 512], P(None, 'tp'), may hold values from -0.125 to 0.125
- shared_down: bfloat16 [512, 2048], P('tp'), may hold values from -0.25 to 0.25
Outputs:
- layer_out: bfloat16 [1024, 2048], P(('grp', 'sp', 'tp')), parts along dimension 0
There are 2 independent parts, one for each index of `grp`. A program takes and returns all parts, laid end to end along the dimension named above; an argument that names none is the same for every part. Nothing has to cross between parts.
Inputs may be any that keep to these rules, and one draw needn't show every extreme that they name: `routes`: in each aligned block of 32 rows (the rows of one device) every row names 6 different experts and no expert is named by more than 24 rows; in every draw some expert is named by exactly 24 rows of every block.
All inputs are finite; a program needn't handle non-finite values.
Results may differ from a plain program's by a relative error of at most 0.015.
Values may be sent and summed in bfloat16 or wider, within the bound.
A program may use at most 64 MiB of HBM per device.

v0:
```python
import functools

import jax
import jax.numpy as jnp
from jax import lax
from jax.experimental import pallas as pl
from jax.experimental.pallas import tpu as pltpu
from jax.sharding import PartitionSpec as P

HEAD = 64
WINDOW = 128
TOPK = 6


norm_eps = 1e-06


def with_halo(block, sides, width):
    for axis, dim in sides:
        count = lax.axis_size(axis)
        forward = [(i, i + 1) for i in range(count - 1)]
        backward = [(target, source) for source, target in forward]
        low = lax.ppermute(
            lax.slice_in_dim(block, block.shape[dim] - width, None, axis=dim), axis, forward
        )
        high = lax.ppermute(lax.slice_in_dim(block, 0, width, axis=dim), axis, backward)
        block = jnp.concatenate([low, block, high], axis=dim)
    return block


def window_attention(query_rows, key_rows, value_rows, sink_logit):
    local_len = query_rows.shape[0]
    head_size = HEAD
    local_kv = key_rows.shape[1] // head_size
    local_heads = query_rows.shape[1] // head_size
    grouped = local_heads // local_kv
    blocks = local_len // WINDOW
    stacked = jnp.stack([key_rows, value_rows])
    widened = with_halo(stacked, (("sp", 1),), WINDOW)
    banded = widened.reshape(2, blocks + 2, WINDOW, local_kv, head_size)
    banded = jnp.concatenate([banded[:, :-2], banded[:, 1:-1], banded[:, 2:]], axis=2)
    queries = query_rows.reshape(blocks, WINDOW, local_kv, grouped, head_size)
    scores = jnp.einsum(
        "nqhgd,nkhd->nhgqk", queries, banded[0], preferred_element_type=jnp.float32
    ) * head_size ** (-0.5)
    seq_start = lax.axis_index("sp") * local_len
    total_len = lax.axis_size("sp") * local_len
    block_ids = jnp.arange(blocks, dtype=jnp.int32)[:, None, None]
    query_pos = seq_start + block_ids * WINDOW + jnp.arange(WINDOW, dtype=jnp.int32)[None, :, None]
    key_pos = (
        seq_start
        + (block_ids - 1) * WINDOW
        + jnp.arange(3 * WINDOW, dtype=jnp.int32)[None, None, :]
    )
    in_window = (jnp.abs(key_pos - query_pos) <= WINDOW) & (key_pos >= 0) & (key_pos < total_len)
    scores = jnp.where(in_window[:, None, None], scores, -jnp.inf)
    sink_part = sink_logit.reshape(1, local_kv, grouped, 1, 1)
    row_max = jnp.maximum(sink_part, jnp.max(scores, axis=-1, keepdims=True))
    shifted = jnp.exp(scores - row_max)
    denominator = jnp.exp(sink_part - row_max) + jnp.sum(shifted, axis=-1, keepdims=True)
    weights = (shifted / denominator).astype(jnp.bfloat16)
    attended = jnp.einsum(
        "nhgqk,nkhd->nqhgd", weights, banded[1], preferred_element_type=jnp.float32
    )
    return attended.astype(jnp.bfloat16).reshape(local_len, local_heads * head_size)


def body(
    query_rows,
    key_rows,
    value_rows,
    sink_logit,
    out_weight,
    residual,
    norm_gain,
    routes,
    gate_weights,
    expert_gate,
    expert_up,
    expert_down,
    shared_gate,
    shared_up,
    shared_down,
):
    attended = window_attention(query_rows, key_rows, value_rows, sink_logit)
    tok_dev = attended.shape[0]
    tok_rows = residual.shape[0]
    model_width = residual.shape[1]
    projected = lax.psum_scatter(
        jnp.dot(attended, out_weight, preferred_element_type=jnp.float32).astype(jnp.bfloat16),
        "tp",
        scatter_dimension=0,
        tiled=True,
    ).astype(jnp.float32)
    stream = residual.astype(jnp.float32) + projected
    normed = (
        stream * lax.rsqrt(jnp.mean(stream * stream, axis=-1, keepdims=True) + norm_eps) * norm_gain
    ).astype(jnp.bfloat16)
    sp_count = lax.axis_size("sp")
    tp_count = lax.axis_size("tp")
    experts_all = sp_count * tp_count
    capacity = (2 * tok_dev * TOPK + tp_count * experts_all - 1) // (tp_count * experts_all)
    copies = tok_rows * TOPK
    flat_expert = routes.reshape(-1)
    one_hot = (flat_expert[:, None] == jnp.arange(experts_all, dtype=jnp.int32)[None, :]).astype(
        jnp.int32
    )
    rank_in_expert = jnp.sum(jnp.cumsum(one_hot, axis=0) * one_hot, axis=1) - 1
    target_slot = flat_expert * capacity + rank_in_expert
    slot_token = (
        jnp.full((experts_all * capacity,), tok_rows, jnp.int32)
        .at[target_slot]
        .set(jnp.arange(copies, dtype=jnp.int32) // TOPK)
    )
    padded_rows = jnp.concatenate([normed, jnp.zeros((1, model_width), jnp.bfloat16)], axis=0)
    outgoing = padded_rows[slot_token].reshape(experts_all, capacity, model_width)
    incoming = lax.all_to_all(outgoing, ("sp", "tp"), split_axis=0, concat_axis=0, tiled=True)
    shaped = incoming.reshape(-1, model_width)
    gate_part = jnp.dot(shaped, expert_gate[0], preferred_element_type=jnp.float32)
    up_part = jnp.dot(shaped, expert_up[0], preferred_element_type=jnp.float32)
    hidden = (jax.nn.silu(gate_part) * up_part).astype(jnp.bfloat16)
    result = jnp.dot(hidden, expert_down[0], preferred_element_type=jnp.float32).astype(
        jnp.bfloat16
    )
    returned = lax.all_to_all(
        result.reshape(incoming.shape), ("sp", "tp"), split_axis=0, concat_axis=0, tiled=True
    )
    returned = returned.reshape(experts_all * capacity, model_width)
    gathered_copies = returned[target_slot].reshape(tok_rows, TOPK, model_width)
    routed = jnp.sum(gate_weights[:, :, None] * gathered_copies.astype(jnp.float32), axis=1)
    slab_rows = lax.all_gather(normed, "tp", axis=0, tiled=True)
    gate_part = jnp.dot(slab_rows, shared_gate, preferred_element_type=jnp.float32)
    up_part = jnp.dot(slab_rows, shared_up, preferred_element_type=jnp.float32)
    hidden = (jax.nn.silu(gate_part) * up_part).astype(jnp.bfloat16)
    partials = jnp.dot(hidden, shared_down, preferred_element_type=jnp.float32)
    shared = lax.psum_scatter(
        partials.astype(jnp.bfloat16), "tp", scatter_dimension=0, tiled=True
    ).astype(jnp.float32)
    return (stream + routed + shared).astype(jnp.bfloat16)


VMEM_BYTES = 66 * 1000 * 1000
PAIR = 2
LANES = 128
CHUNKS = 2


def fused_kernel(
    sp,
    tp,
    q_hbm,
    k_hbm,
    v_hbm,
    sink_ref,
    wo_hbm,
    res_hbm,
    gain_hbm,
    routes_hbm,
    gw_hbm,
    eg_hbm,
    eu_hbm,
    ed_hbm,
    sg_hbm,
    su_hbm,
    sd_hbm,
    out_ref,
    q_v,
    k_v,
    v_v,
    wo_v,
    res_v,
    gain_v,
    routes_v,
    gw_v,
    eg_v,
    eu_v,
    ed_v,
    sg_v,
    su_v,
    sd_v,
    halo_k,
    halo_v,
    att_v,
    proj,
    psend,
    precv,
    pxs,
    pxr,
    stream_v,
    nrm,
    part,
    crecv,
    xsend,
    xrecv,
    zsend,
    zrecv,
    load_sem,
    halo_s,
    halo_r,
    ps_sem,
    pr_sem,
    s_core,
    s_x,
    s_up,
    s_dn,
    nrm_r,
    cs_sem,
    cr_sem,
    xs_sem,
    xr_sem,
    zs_sem,
    zr_sem,
):
    z = lax.axis_index("sp")
    t = lax.axis_index("tp")
    c = t % PAIR
    x = t // PAIR
    t_core = x * PAIR + (1 - c)
    t_x = (1 - x) * PAIR + c
    t_far = (1 - x) * PAIR + (1 - c)
    core = {"tp": t_core}
    xnbr = {"tp": t_x}

    def at_z(pos):
        return {"sp": pos}

    def rcopy(src, dst, ssem, rsem, dev):
        return pltpu.make_async_remote_copy(
            src_ref=src,
            dst_ref=dst,
            send_sem=ssem,
            recv_sem=rsem,
            device_id=dev,
            device_id_type=pl.DeviceIdType.MESH,
        )

    moves = [
        (k_hbm, k_v),
        (v_hbm, v_v),
        (q_hbm, q_v),
        (wo_hbm, wo_v),
        (res_hbm, res_v),
        (gain_hbm, gain_v),
        (routes_hbm, routes_v),
        (gw_hbm, gw_v),
        (sg_hbm, sg_v),
        (su_hbm, su_v),
        (sd_hbm, sd_v),
        (eg_hbm.at[0], eg_v),
        (eu_hbm.at[0], eu_v),
        (ed_hbm.at[0], ed_v),
    ]
    loads = [pltpu.make_async_copy(a, b, load_sem.at[i]) for i, (a, b) in enumerate(moves)]
    barrier = pltpu.get_barrier_semaphore()
    for dev in (core, xnbr):
        pl.semaphore_signal(barrier, inc=1, device_id=dev, device_id_type=pl.DeviceIdType.MESH)
    @pl.when(z > 0)
    def _():
        pl.semaphore_signal(
            barrier, inc=1, device_id=at_z(z - 1), device_id_type=pl.DeviceIdType.MESH
        )

    @pl.when(z < sp - 1)
    def _():
        pl.semaphore_signal(
            barrier, inc=1, device_id=at_z(z + 1), device_id_type=pl.DeviceIdType.MESH
        )

    for load in loads:
        load.start()
    rows = stream_v.shape[0]
    width = stream_v.shape[1]
    length = q_v.shape[0]
    heads = q_v.shape[1] // HEAD
    grouped = heads // (k_v.shape[1] // HEAD)

    @pl.when(z == 0)
    def _():
        halo_k[0] = jnp.zeros(halo_k.shape[1:], halo_k.dtype)
        halo_v[0] = jnp.zeros(halo_v.shape[1:], halo_v.dtype)

    @pl.when(z == sp - 1)
    def _():
        halo_k[1] = jnp.zeros(halo_k.shape[1:], halo_k.dtype)
        halo_v[1] = jnp.zeros(halo_v.shape[1:], halo_v.dtype)

    loads[0].wait()
    loads[1].wait()
    peers = 2 + jnp.where(z > 0, 1, 0) + jnp.where(z < sp - 1, 1, 0)
    pl.semaphore_wait(barrier, peers)

    def halo(up):
        pos = z + 1 if up else z - 1
        slot = 0 if up else 1
        row = 0 if up else 1
        return (
            rcopy(k_v, halo_k.at[slot], halo_s.at[row, 0], halo_r.at[slot, 0], at_z(pos)),
            rcopy(v_v, halo_v.at[slot], halo_s.at[row, 1], halo_r.at[slot, 1], at_z(pos)),
        )

    @pl.when(z < sp - 1)
    def _():
        for copy in halo(True):
            copy.start()

    @pl.when(z > 0)
    def _():
        for copy in halo(False):
            copy.start()

    loads[6].wait()
    loads[7].wait()
    half = LANES // 2
    lane = lax.broadcasted_iota(jnp.int32, (rows, LANES), 1)
    unit = lax.broadcasted_iota(jnp.int32, (LANES, rows), 0)
    unit = jnp.where(unit < half, unit, unit - half)
    combine = jnp.zeros((LANES, rows), jnp.float32)
    for k in range(TOPK):
        combine = combine + jnp.where(routes_v[k : k + 1] == unit, gw_v[k : k + 1], 0.0)
    combine = combine.T
    high = combine.astype(jnp.bfloat16)
    low = (combine - high.astype(jnp.float32)).astype(jnp.bfloat16)
    nrm[z, t, :, width:] = jnp.where(
        lane < half, high.astype(jnp.float32), low.astype(jnp.float32)
    ).astype(jnp.bfloat16)

    loads[2].wait()
    contract = (((1,), (1,)), ((), ()))
    scale = HEAD ** (-0.5)

    def cols(head):
        return slice(head * HEAD, (head + 1) * HEAD)

    own_scores = []
    for head in range(heads):
        own_scores.append(
            lax.dot_general(
                q_v[:, cols(head)],
                k_v[:, cols(head // grouped)],
                contract,
                preferred_element_type=jnp.float32,
            )
            * scale
        )

    @pl.when(z > 0)
    def _():
        for copy in (
            rcopy(k_v, halo_k.at[0], halo_s.at[0, 0], halo_r.at[0, 0], core),
            rcopy(v_v, halo_v.at[0], halo_s.at[0, 1], halo_r.at[0, 1], core),
        ):
            copy.wait_recv()

    @pl.when(z < sp - 1)
    def _():
        for copy in (
            rcopy(k_v, halo_k.at[1], halo_s.at[1, 0], halo_r.at[1, 0], core),
            rcopy(v_v, halo_v.at[1], halo_s.at[1, 1], halo_r.at[1, 1], core),
        ):
            copy.wait_recv()

    qi = lax.broadcasted_iota(jnp.int32, (length, length), 0)
    ki = lax.broadcasted_iota(jnp.int32, (length, length), 1)
    low_bound = jnp.where(z > 0, 0, length)
    high_bound = jnp.where(z < sp - 1, 0, length)
    low_mask = ki - qi >= low_bound
    high_mask = qi - ki >= high_bound
    for head in range(heads):
        kv = cols(head // grouped)
        qh = q_v[:, cols(head)]
        s_own = own_scores[head]
        s_low = jnp.where(
            low_mask,
            lax.dot_general(qh, halo_k[0, :, kv], contract, preferred_element_type=jnp.float32)
            * scale,
            -jnp.inf,
        )
        s_high = jnp.where(
            high_mask,
            lax.dot_general(qh, halo_k[1, :, kv], contract, preferred_element_type=jnp.float32)
            * scale,
            -jnp.inf,
        )
        sink = sink_ref[head]
        top = jnp.max(
            jnp.maximum(jnp.maximum(s_low, s_high), s_own), axis=-1, keepdims=True
        )
        top = jnp.maximum(top, sink)
        e_low = jnp.exp(s_low - top)
        e_own = jnp.exp(s_own - top)
        e_high = jnp.exp(s_high - top)
        denominator = jnp.exp(sink - top) + jnp.sum(e_low + e_own + e_high, axis=-1, keepdims=True)
        inverse = 1.0 / denominator
        attended = jnp.dot(
            (e_own * inverse).astype(jnp.bfloat16), v_v[:, kv], preferred_element_type=jnp.float32
        )
        attended += jnp.dot(
            (e_low * inverse).astype(jnp.bfloat16),
            halo_v[0, :, kv],
            preferred_element_type=jnp.float32,
        )
        attended += jnp.dot(
            (e_high * inverse).astype(jnp.bfloat16),
            halo_v[1, :, kv],
            preferred_element_type=jnp.float32,
        )
        att_v[:, cols(head)] = attended.astype(jnp.bfloat16)

    loads[3].wait()
    proj[...] = jnp.dot(
        att_v[...], wo_v[...], preferred_element_type=jnp.float32
    ).reshape(proj.shape)
    piece = rows // CHUNKS

    def cut(j):
        return pl.ds(j * piece, piece)

    pcore = []
    for order, xx in enumerate((1 - x, x)):
        psend[xx] = proj[xx * PAIR + (1 - c)].astype(jnp.bfloat16)
        pcore.append(rcopy(psend.at[xx], precv.at[xx], ps_sem.at[order], pr_sem.at[order], core))
        pcore[-1].start()
    pcore[0].wait_recv()
    pcross = []
    for j in range(CHUNKS):
        pxs[cut(j)] = (proj[t_x, cut(j)] + precv[1 - x, cut(j)].astype(jnp.float32)).astype(
            jnp.bfloat16
        )
        pcross.append(
            rcopy(
                pxs.at[cut(j)], pxr.at[cut(j)], ps_sem.at[PAIR + j], pr_sem.at[PAIR + j], xnbr
            )
        )
        pcross[-1].start()
    loads[4].wait()
    loads[5].wait()
    pcore[1].wait_recv()
    stream_v[...] = res_v[...].astype(jnp.float32) + proj[t] + precv[x].astype(jnp.float32)

    def carry(g, tt, j, ssem, dev):
        ref = nrm.at[g, tt, cut(j)]
        return rcopy(ref, ref, ssem, nrm_r.at[g, tt, j], dev)

    def to_core(g, tt, j):
        return carry(g, tt, j, s_core.at[g, tt, j], core)

    def to_x(g, j):
        return carry(g, t, j, s_x.at[g, j], xnbr)

    def to_up(g, j):
        return carry(g, t, j, s_up.at[g, j], at_z(z + 1))

    def to_dn(g, j):
        return carry(g, t, j, s_dn.at[g, j], at_z(z - 1))

    def nrm_wait(g, tt, j):
        to_core(g, tt, j).wait_recv()

    below = z
    above = sp - 1 - z
    short = jnp.minimum(below, above)

    def group_of(i):
        if i < 0:
            return z
        paired = i < 2 * short
        dist = jnp.where(paired, i // 2 + 1, i - short + 1)
        if i % 2 == 0:
            sign_pair = -1
        else:
            sign_pair = 1
        sign = jnp.where(paired, sign_pair, jnp.where(below > above, -1, 1))
        return z + sign * dist

    groups = {i: group_of(i) for i in range(-1, sp - 1)}

    def stage_a(i, j):
        g = groups[i]
        if i >= 0:
            nrm_wait(g, t, j)

        @pl.when((g <= z) & (z < sp - 1))
        def _():
            to_up(g, j).start()

        @pl.when((g >= z) & (z > 0))
        def _():
            to_dn(g, j).start()

        to_x(g, j).start()
        to_core(g, t, j).start()

    def stage_b(i, j):
        g = groups[i]
        nrm_wait(g, t_x, j)
        to_core(g, t_x, j).start()

    def stage_c(i):
        g = groups[i]
        for j in range(CHUNKS):
            nrm_wait(g, t_core, j)
            nrm_wait(g, t_far, j)

    expert = z * tp + t

    def part_send(g):
        return rcopy(part.at[g, 1 - c], crecv.at[g], cs_sem.at[g], cr_sem.at[g], core)

    def cross_send(g, j):
        return rcopy(
            xsend.at[g, cut(j)], xrecv.at[g, cut(j)], xs_sem.at[g, j], xr_sem.at[g, j], xnbr
        )

    def line_send(g, j):
        return rcopy(
            zsend.at[g, cut(j)], zrecv.at[z, cut(j)], zs_sem.at[g, j], zr_sem.at[z, j], at_z(g)
        )

    def silu(v):
        return v / (1.0 + jnp.exp(-v))

    def stage_d(i):
        g = groups[i]
        if i < 0:
            for k in range(8, 14):
                loads[k].wait()
        block = nrm[g].reshape(tp * rows, nrm.shape[-1])
        acts = block[:, :width]
        tail = block[:, width:].astype(jnp.float32)
        lanes = lax.broadcasted_iota(jnp.int32, tail.shape, 1)
        mine = (lanes == expert) | (lanes == expert + half)
        weight = jnp.sum(jnp.where(mine, tail, 0.0), axis=-1, keepdims=True)
        gate = jnp.dot(acts, eg_v[...], preferred_element_type=jnp.float32)
        up = jnp.dot(acts, eu_v[...], preferred_element_type=jnp.float32)
        hidden = (silu(gate) * up).astype(jnp.bfloat16)
        result = jnp.dot(hidden, ed_v[...], preferred_element_type=jnp.float32)
        result = weight * result.astype(jnp.bfloat16).astype(jnp.float32)
        if i < 0:
            gate = jnp.dot(acts, sg_v[...], preferred_element_type=jnp.float32)
            up = jnp.dot(acts, su_v[...], preferred_element_type=jnp.float32)
            hidden = (silu(gate) * up).astype(jnp.bfloat16)
            shared = jnp.dot(hidden, sd_v[...], preferred_element_type=jnp.float32)
            result = result + shared.astype(jnp.bfloat16).astype(jnp.float32)
        result = result.astype(jnp.bfloat16)
        for tt in range(tp):
            part[g, tt % PAIR, tt // PAIR] = result[tt * rows : (tt + 1) * rows]
        part_send(g).start()

    def stage_e(i):
        g = groups[i]
        part_send(g).wait_recv()
        for j in range(CHUNKS):
            xsend[g, cut(j)] = (
                part[g, c, 1 - x, cut(j)].astype(jnp.float32)
                + crecv[g, 1 - x, cut(j)].astype(jnp.float32)
            ).astype(jnp.bfloat16)
            cross_send(g, j).start()

    def column(g, j):
        cross_send(g, j).wait_recv()
        return (
            part[g, c, x, cut(j)].astype(jnp.float32)
            + crecv[g, x, cut(j)].astype(jnp.float32)
            + xrecv[g, cut(j)].astype(jnp.float32)
        )

    def stage_f(i):
        g = groups[i]
        for j in range(CHUNKS):
            zsend[g, cut(j)] = column(g, j).astype(jnp.bfloat16)
            line_send(g, j).start()

    last = sp - 2

    def relay(i):
        for j in range(CHUNKS):
            if i <= last:
                stage_a(i, j)
            if i - 1 <= last:
                stage_b(i - 1, j)

    for j in range(CHUNKS):
        pcross[j].wait_recv()
        stream = stream_v[cut(j)] + pxr[cut(j)].astype(jnp.float32)
        stream_v[cut(j)] = stream
        nrm[z, t, cut(j), :width] = (
            stream
            * lax.rsqrt(jnp.mean(stream * stream, axis=-1, keepdims=True) + norm_eps)
            * gain_v[...]
        ).astype(jnp.bfloat16)
        stage_a(-1, j)

    @pl.when(short > 0)
    def _():
        for j in range(CHUNKS):
            for i in range(min(2, last + 1)):
                stage_a(i, j)
            stage_b(-1, j)
        for i in range(2, last + 1):
            for j in range(CHUNKS):
                stage_a(i, j)
        for j in range(CHUNKS):
            stage_b(0, j)

    @pl.when(short == 0)
    def _():
        relay(0)
        relay(1)

    stage_c(-1)
    stage_d(-1)
    for i in range(last + 1):
        if i + 2 <= last:

            @pl.when(short == 0)
            def _():
                for j in range(CHUNKS):
                    stage_a(i + 2, j)

        stage_c(i)
        stage_d(i)
        if i + 1 <= last:
            for j in range(CHUNKS):
                stage_b(i + 1, j)
        if i == last and i > 0:
            stage_f(0)
        stage_e(i)
    stage_e(-1)
    for i in range(0 if last == 0 else 1, last + 1):
        stage_f(i)
    @pl.when(z < sp - 1)
    def _():
        for copy in halo(True):
            copy.wait_send()

    @pl.when(z > 0)
    def _():
        for copy in halo(False):
            copy.wait_send()

    for copy in pcore + pcross:
        copy.wait_send()
    for i in range(-1, sp - 1):
        g = groups[i]
        part_send(g).wait_send()
        for j in range(CHUNKS):

            @pl.when((g <= z) & (z < sp - 1))
            def _():
                to_up(g, j).wait_send()

            @pl.when((g >= z) & (z > 0))
            def _():
                to_dn(g, j).wait_send()

            to_x(g, j).wait_send()
            to_core(g, t, j).wait_send()
            to_core(g, t_x, j).wait_send()
            if i >= 0:
                cross_send(g, j).wait_send()
            if 0 <= i < last:
                line_send(g, j).wait_send()

    for j in range(CHUNKS):
        stream_v[cut(j)] = stream_v[cut(j)] + column(z, j)
    for step in range(1, sp):
        src = groups[step - 1]
        for j in range(CHUNKS):
            rcopy(
                zsend.at[src, cut(j)],
                zrecv.at[src, cut(j)],
                zs_sem.at[src, j],
                zr_sem.at[src, j],
                at_z(src),
            ).wait_recv()
            total = stream_v[cut(j)] + zrecv[src, cut(j)].astype(jnp.float32)
            if step < sp - 1:
                stream_v[cut(j)] = total
            else:
                out_ref[cut(j)] = total.astype(out_ref.dtype)
    for j in range(CHUNKS):
        cross_send(z, j).wait_send()
        line_send(groups[last], j).wait_send()


def fused_scratch(sp, tp, shapes):
    (q, k, v, _, wo, res, gain, routes, gw, eg, eu, ed, sg, su, sd) = shapes
    rows, width = res.shape
    bf = jnp.bfloat16
    f32 = jnp.float32
    cross = tp // PAIR
    return [
        (q.shape, bf),
        (k.shape, bf),
        (v.shape, bf),
        (wo.shape, bf),
        (res.shape, bf),
        (gain.shape, f32),
        (routes.shape, jnp.int32),
        (gw.shape, f32),
        (eg.shape[1:], bf),
        (eu.shape[1:], bf),
        (ed.shape[1:], bf),
        (sg.shape, bf),
        (su.shape, bf),
        (sd.shape, bf),
        ((2,) + k.shape, bf),
        ((2,) + v.shape, bf),
        (q.shape, bf),
        ((tp, rows, width), f32),
        ((cross, rows, width), bf),
        ((cross, rows, width), bf),
        ((rows, width), bf),
        ((rows, width), bf),
        ((rows, width), f32),
        ((sp, tp, rows, width + LANES), bf),
        ((sp, PAIR, cross, rows, width), bf),
        ((sp, cross, rows, width), bf),
        ((sp, rows, width), bf),
        ((sp, rows, width), bf),
        ((sp, rows, width), bf),
        ((sp, rows, width), bf),
    ]


def size_of(shape, dtype):
    total = jnp.dtype(dtype).itemsize
    for extent in shape:
        total *= extent
    return total


def fused(sp, tp, buffers, *args):
    dma = pltpu.SemaphoreType.DMA
    any_spec = pl.BlockSpec(memory_space=pltpu.HBM)
    specs = [any_spec] * 15
    specs[3] = pl.BlockSpec(memory_space=pltpu.SMEM)
    res = args[5]
    return pl.pallas_call(
        functools.partial(fused_kernel, sp, tp),
        out_shape=jax.ShapeDtypeStruct(res.shape, jnp.bfloat16),
        in_specs=specs,
        out_specs=pl.BlockSpec(memory_space=pltpu.VMEM),
        scratch_shapes=[pltpu.VMEM(s, d) for s, d in buffers]
        + [
            dma((14,)),
            dma((2, 2)),
            dma((2, 2)),
            dma((PAIR + CHUNKS,)),
            dma((PAIR + CHUNKS,)),
            dma((sp, tp, CHUNKS)),
            dma((sp, CHUNKS)),
            dma((sp, CHUNKS)),
            dma((sp, CHUNKS)),
            dma((sp, tp, CHUNKS)),
            dma((sp,)),
            dma((sp,)),
            dma((sp, CHUNKS)),
            dma((sp, CHUNKS)),
            dma((sp, CHUNKS)),
            dma((sp, CHUNKS)),
        ],
        compiler_params=pltpu.CompilerParams(
            collective_id=0, has_side_effects=True, vmem_limit_bytes=VMEM_BYTES
        ),
    )(*args)


def either(*args):
    sp = lax.axis_size("sp")
    tp = lax.axis_size("tp")
    args = list(args)
    shaped = list(args)
    shaped[6] = args[6].reshape(1, -1)
    shaped[7] = args[7].T
    shaped[8] = args[8].T
    buffers = fused_scratch(sp, tp, shaped)
    needed = sum(size_of(s, d) for s, d in buffers)
    fits = (
        2 * needed <= VMEM_BYTES
        and tp == 2 * PAIR
        and sp > 1
        and args[5].shape[0] % (16 * CHUNKS) == 0
        and 2 * sp * tp <= LANES
        and args[0].shape[0] == WINDOW
        and args[9].shape[0] == 1
    )
    if fits:
        return fused(sp, tp, buffers, *shaped)
    return body(*args)


def solution(mesh):
    placed = (
        P(("grp", "sp"), "tp"),
        P(("grp", "sp"), "tp"),
        P(("grp", "sp"), "tp"),
        P("tp"),
        P("tp", None),
        P(("grp", "sp", "tp"), None),
        P(),
        P(("grp", "sp", "tp"), None),
        P(("grp", "sp", "tp"), None),
        P(("sp", "tp"), None, None),
        P(("sp", "tp"), None, None),
        P(("sp", "tp"), None, None),
        P(None, "tp"),
        P(None, "tp"),
        P("tp", None),
    )
    return jax.shard_map(
        either, mesh=mesh, in_specs=placed, out_specs=P(("grp", "sp", "tp"), None), check_vma=False
    )
```

profile of v0, /device:TPU:0, one launch (start us, length us, event | category | flops | bytes accessed | tf_op | source)
XLA Modules:
  0.0 49.8 jit_solution(2117480947788036894)
XLA Ops:
  0.0 48.2 %shard_map.145 = bf16[32,2048]{1,0:T(8,128)(2,1)} custom-call(bf16[128,256]{1,0:T(8,128)(2,1)} %q_hbm.1, bf16[128,128]{1,0:T(8,128)(2,1)} %k_hbm.1, bf16[128,128]{1,0:T(8,128)(2,1)} %v_hbm.1, f32[4]{0:T(128)} %sink_ref.1, bf16[256,2048]{1,0:T(8,128)(2,1)} %wo_hbm.1, bf16[32,2048]{1,0:T(8,128)(2,1)} %res_hbm.1, f32[1,2048]{1,0:T(1,128)} %bitcast.3, ...), custom_call_target="tpu_custom_call" | custom-call | tf_op jit(solution)/shard_map/pallas_call | solution.py:739
  48.3 1.6 %copy.17 = bf16[32,2048]{1,0:T(8,128)(2,1)} copy(bf16[32,2048]{1,0:T(8,128)(2,1)} %shard_map.145) | data formatting | bytes 262144
where the time goes:
time: 50 us; the launch traced here: 49.8 us
  Pallas kernels  48.2 us (96%)
  local copies, waits for them, and re-layouts  1.57 us (3%)
    pallas_call x1, Pallas kernels, fused(): pl.pallas_call(functools.partial(fused_kernel, sp, tp), out_shape=jax.Sha...  48.2 us
    unnamed x1, local copies, waits for them, and re-layouts  1.57 us

commit v1 on v0

--- a/solution.py
+++ b/solution.py
@@ -738,7 +738,7 @@
     res = args[5]
     return pl.pallas_call(
         functools.partial(fused_kernel, sp, tp),
-        out_shape=jax.ShapeDtypeStruct(res.shape, jnp.bfloat16),
+        out_shape=pltpu.VMEM(res.shape, jnp.bfloat16),
         in_specs=specs,
         out_specs=pl.BlockSpec(memory_space=pltpu.VMEM),
         scratch_shapes=[pltpu.VMEM(s, d) for s, d in buffers]

time: 50 us -> 48.4 us (0.968)
  local copies, waits for them, and re-layouts: 1.57 us -> 0.66 us
  Pallas kernels: 48.2 us -> 47.6 us
    unnamed x1, local copies, waits for them, and re-layouts: 1.57 us -> 0.66 us
    pallas_call x1, Pallas kernels: 48.2 us -> 47.6 us  [fused(): pl.pallas_call(functools.partial(fused_kernel, sp, tp), out_shape=pltpu.V...]
where the time goes in v1:
time: 48.4 us; the launch traced here: 48.3 us
  Pallas kernels  47.6 us (98%)
  local copies, waits for them, and re-layouts  0.66 us (1%)
    pallas_call x1, Pallas kernels, fused(): pl.pallas_call(functools.partial(fused_kernel, sp, tp), out_shape=pltpu.V...  47.6 us

profile of v1, /device:TPU:0, one launch (start us, length us, event | category | flops | bytes accessed | tf_op | source)
XLA Modules:
  0.0 48.3 jit_solution(7161965396810288571)
XLA Ops:
  0.0 47.6 %shard_map.145 = bf16[32,2048]{1,0:T(8,128)(2,1)S(1)} custom-call(bf16[128,256]{1,0:T(8,128)(2,1)} %q_hbm.1, bf16[128,128]{1,0:T(8,128)(2,1)} %k_hbm.1, bf16[128,128]{1,0:T(8,128)(2,1)} %v_hbm.1, f32[4]{0:T(128)} %sink_ref.1, bf16[256,2048]{1,0:T(8,128)(2,1)} %wo_hbm.1, bf16[32,2048]{1,0:T(8,128)(2,1)} %res_hbm.1, f32[1,2048]{1,0:T(1,128)} %bitcast.3, ...), custom_call_target="tpu_custom_call" | custom-call | tf_op jit(solution)/shard_map/pallas_call | solution.py:739
  47.6 0.7 %copy.17 = bf16[32,2048]{1,0:T(8,128)(2,1)} copy(bf16[32,2048]{1,0:T(8,128)(2,1)S(1)} %shard_map.145) | data formatting | bytes 262144

commit v2 on v1

v2 whole, which is shorter than its diff:
```python
import functools

import jax
import jax.numpy as jnp
from jax import lax
from jax.experimental import pallas as pl
from jax.experimental.pallas import tpu as pltpu
from jax.sharding import PartitionSpec as P

HEAD = 64
WINDOW = 128
TOPK = 6


norm_eps = 1e-06


def with_halo(block, sides, width):
    for axis, dim in sides:
        count = lax.axis_size(axis)
        forward = [(i, i + 1) for i in range(count - 1)]
        backward = [(target, source) for source, target in forward]
        low = lax.ppermute(
            lax.slice_in_dim(block, block.shape[dim] - width, None, axis=dim), axis, forward
        )
        high = lax.ppermute(lax.slice_in_dim(block, 0, width, axis=dim), axis, backward)
        block = jnp.concatenate([low, block, high], axis=dim)
    return block


def window_attention(query_rows, key_rows, value_rows, sink_logit):
    local_len = query_rows.shape[0]
    head_size = HEAD
    local_kv = key_rows.shape[1] // head_size
    local_heads = query_rows.shape[1] // head_size
    grouped = local_heads // local_kv
    blocks = local_len // WINDOW
    stacked = jnp.stack([key_rows, value_rows])
    widened = with_halo(stacked, (("sp", 1),), WINDOW)
    banded = widened.reshape(2, blocks + 2, WINDOW, local_kv, head_size)
    banded = jnp.concatenate([banded[:, :-2], banded[:, 1:-1], banded[:, 2:]], axis=2)
    queries = query_rows.reshape(blocks, WINDOW, local_kv, grouped, head_size)
    scores = jnp.einsum(
        "nqhgd,nkhd->nhgqk", queries, banded[0], preferred_element_type=jnp.float32
    ) * head_size ** (-0.5)
    seq_start = lax.axis_index("sp") * local_len
    total_len = lax.axis_size("sp") * local_len
    block_ids = jnp.arange(blocks, dtype=jnp.int32)[:, None, None]
    query_pos = seq_start + block_ids * WINDOW + jnp.arange(WINDOW, dtype=jnp.int32)[None, :, None]
    key_pos = (
        seq_start
        + (block_ids - 1) * WINDOW
        + jnp.arange(3 * WINDOW, dtype=jnp.int32)[None, None, :]
    )
    in_window = (jnp.abs(key_pos - query_pos) <= WINDOW) & (key_pos >= 0) & (key_pos < total_len)
    scores = jnp.where(in_window[:, None, None], scores, -jnp.inf)
    sink_part = sink_logit.reshape(1, local_kv, grouped, 1, 1)
    row_max = jnp.maximum(sink_part, jnp.max(scores, axis=-1, keepdims=True))
    shifted = jnp.exp(scores - row_max)
    denominator = jnp.exp(sink_part - row_max) + jnp.sum(shifted, axis=-1, keepdims=True)
    weights = (shifted / denominator).astype(jnp.bfloat16)
    attended = jnp.einsum(
        "nhgqk,nkhd->nqhgd", weights, banded[1], preferred_element_type=jnp.float32
    )
    return attended.astype(jnp.bfloat16).reshape(local_len, local_heads * head_size)


def body(
    query_rows,
    key_rows,
    value_rows,
    sink_logit,
    out_weight,
    residual,
    norm_gain,
    routes,
    gate_weights,
    expert_gate,
    expert_up,
    expert_down,
    shared_gate,
    shared_up,
    shared_down,
):
    attended = window_attention(query_rows, key_rows, value_rows, sink_logit)
    tok_dev = attended.shape[0]
    tok_rows = residual.shape[0]
    model_width = residual.shape[1]
    projected = lax.psum_scatter(
        jnp.dot(attended, out_weight, preferred_element_type=jnp.float32).astype(jnp.bfloat16),
        "tp",
        scatter_dimension=0,
        tiled=True,
    ).astype(jnp.float32)
    stream = residual.astype(jnp.float32) + projected
    normed = (
        stream * lax.rsqrt(jnp.mean(stream * stream, axis=-1, keepdims=True) + norm_eps) * norm_gain
    ).astype(jnp.bfloat16)
    sp_count = lax.axis_size("sp")
    tp_count = lax.axis_size("tp")
    experts_all = sp_count * tp_count
    capacity = (2 * tok_dev * TOPK + tp_count * experts_all - 1) // (tp_count * experts_all)
    copies = tok_rows * TOPK
    flat_expert = routes.reshape(-1)
    one_hot = (flat_expert[:, None] == jnp.arange(experts_all, dtype=jnp.int32)[None, :]).astype(
        jnp.int32
    )
    rank_in_expert = jnp.sum(jnp.cumsum(one_hot, axis=0) * one_hot, axis=1) - 1
    target_slot = flat_expert * capacity + rank_in_expert
    slot_token = (
        jnp.full((experts_all * capacity,), tok_rows, jnp.int32)
        .at[target_slot]
        .set(jnp.arange(copies, dtype=jnp.int32) // TOPK)
    )
    padded_rows = jnp.concatenate([normed, jnp.zeros((1, model_width), jnp.bfloat16)], axis=0)
    outgoing = padded_rows[slot_token].reshape(experts_all, capacity, model_width)
    incoming = lax.all_to_all(outgoing, ("sp", "tp"), split_axis=0, concat_axis=0, tiled=True)
    shaped = incoming.reshape(-1, model_width)
    gate_part = jnp.dot(shaped, expert_gate[0], preferred_element_type=jnp.float32)
    up_part = jnp.dot(shaped, expert_up[0], preferred_element_type=jnp.float32)
    hidden = (jax.nn.silu(gate_part) * up_part).astype(jnp.bfloat16)
    result = jnp.dot(hidden, expert_down[0], preferred_element_type=jnp.float32).astype(
        jnp.bfloat16
    )
    returned = lax.all_to_all(
        result.reshape(incoming.shape), ("sp", "tp"), split_axis=0, concat_axis=0, tiled=True
    )
    returned = returned.reshape(experts_all * capacity, model_width)
    gathered_copies = returned[target_slot].reshape(tok_rows, TOPK, model_width)
    routed = jnp.sum(gate_weights[:, :, None] * gathered_copies.astype(jnp.float32), axis=1)
    slab_rows = lax.all_gather(normed, "tp", axis=0, tiled=True)
    gate_part = jnp.dot(slab_rows, shared_gate, preferred_element_type=jnp.float32)
    up_part = jnp.dot(slab_rows, shared_up, preferred_element_type=jnp.float32)
    hidden = (jax.nn.silu(gate_part) * up_part).astype(jnp.bfloat16)
    partials = jnp.dot(hidden, shared_down, preferred_element_type=jnp.float32)
    shared = lax.psum_scatter(
        partials.astype(jnp.bfloat16), "tp", scatter_dimension=0, tiled=True
    ).astype(jnp.float32)
    return (stream + routed + shared).astype(jnp.bfloat16)


VMEM_BYTES = 66 * 1000 * 1000
PAIR = 2
LINE = 4
LANES = 128
CHUNKS = 2
SENDS = 20
DISPATCH_BY_LINE = ((0, 1),)
RETURN_BY_LINE = ((0, 2), (1, 0),)
RELAYS = {(0, 3): 2, (1, 3): 2}
ADDERS = {}
ORDER = {
    0: (
        ("N", 0),
        ("S", "o", 1, 0),
        ("N", 1),
        ("M", 0),
        ("S", "o", 2, 0),
        ("A", 1, "o", 0),
        ("M", 1),
        ("S", "o", 3, 0),
        ("S", "o", 2, 1),
        ("S", "m", 2, 0),
        ("S", "o", 3, 1),
        ("Q", 0),
        ("A", 1, "o", 1),
        ("S", "m", 1, 0),
        ("S", "m", 1, 1),
        ("S", "m", 2, 1),
        ("A", 2, "o", 0),
        ("Q", 2),
        ("A", 2, "o", 1),
        ("S", "o", 1, 1),
        ("A", 3, "o", 0),
        ("A", 3, "o", 1),
        ("A", 2, "m", 1),
        ("A", 1, "m", 0),
        ("A", 1, "m", 1),
        ("A", 2, "m", 0),
        ("S", "m", 3, 1),
        ("D", (1, 2)),
        ("E", 2),
        ("A", 3, "m", 1),
        ("A", 3, "m", 0),
        ("E", 1),
        ("D", (3,)),
        ("E", 3),
        ("S", "m", 3, 0),
        ("F", 3, 0),
        ("F", 3, 1),
        ("F", 1, 1),
        ("F", 1, 0),
        ("Q", 1),
        ("E", 0),
        ("F", 2, 1),
        ("G", 2, 1),
        ("H", 1),
        ("G", 3, 0),
        ("G", 1, 1),
        ("F", 2, 0),
        ("G", 1, 0),
        ("H", 0),
        ("G", 2, 0),
        ("G", 3, 1),
    ),
    1: (
        ("N", 0),
        ("S", "o", 2, 0),
        ("S", "o", 0, 0),
        ("N", 1),
        ("S", "o", 0, 1),
        ("S", "o", 3, 0),
        ("S", "o", 2, 1),
        ("M", 0),
        ("M", 1),
        ("A", 0, "o", 0),
        ("A", 2, "o", 0),
        ("S", "m", 2, 0),
        ("Q", 0),
        ("A", 2, "o", 1),
        ("A", 3, "o", 0),
        ("A", 3, "o", 1),
        ("A", 2, "m", 1),
        ("A", 0, "o", 1),
        ("A", 3, "m", 1),
        ("A", 0, "m", 0),
        ("A", 3, "m", 0),
        ("A", 2, "m", 0),
        ("A", 0, "m", 1),
        ("D", (0, 2, 3)),
        ("E", 2),
        ("E", 0),
        ("Q", 2),
        ("S", "m", 3, 1),
        ("Q", 1),
        ("S", "m", 0, 1),
        ("S", "o", 3, 1),
        ("F", 2, 0),
        ("E", 3),
        ("F", 0, 0),
        ("F", 3, 1),
        ("S", "m", 2, 1),
        ("F", 3, 0),
        ("S", "m", 0, 0),
        ("S", "m", 3, 0),
        ("E", 1),
        ("F", 2, 1),
        ("H", 0),
        ("H", 1),
        ("G", 0, 1),
        ("G", 3, 0),
        ("F", 0, 1),
        ("G", 2, 0),
        ("G", 2, 1),
        ("G", 3, 1),
        ("G", 0, 0),
    ),
}


def listed(source, target, pairs):
    mirrored = (LINE - 1 - source, LINE - 1 - target)
    return (source, target) in pairs or mirrored in pairs


def relay_of(source, target):
    if (source, target) in RELAYS:
        return RELAYS[(source, target)]
    mirrored = (LINE - 1 - source, LINE - 1 - target)
    if mirrored in RELAYS:
        return LINE - 1 - RELAYS[mirrored]
    return None


def adder_of(source, target):
    if listed(source, target, RETURN_BY_LINE):
        return None
    mirrored = (LINE - 1 - source, LINE - 1 - target)
    if (source, target) in ADDERS:
        adder = ADDERS[(source, target)]
    elif mirrored in ADDERS:
        adder = LINE - 1 - ADDERS[mirrored]
    else:
        return None
    return None if listed(adder, target, RETURN_BY_LINE) else adder


def silu(v):
    return v / (1.0 + jnp.exp(-v))


def fused_kernel(
    sp,
    tp,
    q_hbm,
    k_hbm,
    v_hbm,
    sink_hbm,
    wo_hbm,
    res_hbm,
    gain_hbm,
    routes_hbm,
    gw_hbm,
    eg_hbm,
    eu_hbm,
    ed_hbm,
    sg_hbm,
    su_hbm,
    sd_hbm,
    out_ref,
    q_v,
    k_v,
    v_v,
    sink_s,
    wo_v,
    res_v,
    gain_v,
    routes_v,
    gw_v,
    eg_v,
    eu_v,
    ed_v,
    sg_v,
    su_v,
    sd_v,
    eg_o,
    eu_o,
    ed_o,
    sg_o,
    su_o,
    sd_o,
    halo_k,
    halo_v,
    att_v,
    proj,
    psend,
    precv,
    pxs,
    pxr,
    pys,
    pyr,
    stream_v,
    mirror_v,
    tail_s,
    tail_m,
    nrm,
    part,
    xsend,
    xrecv,
    zsend,
    zrecv,
    zadd,
    load_sem,
    halo_r,
    pr_sem,
    w_s,
    w_r,
    send_sem,
    nrm_r,
    xr_sem,
    zr_sem,
    za_sem,
    far_sem,
):
    z = lax.axis_index("sp")
    t = lax.axis_index("tp")
    c = t % PAIR
    x = t // PAIR
    t_core = x * PAIR + (1 - c)
    t_x = (1 - x) * PAIR + c
    core = {"tp": t_core}
    xnbr = {"tp": t_x}
    upper = z // (sp // 2)

    def at_z(pos):
        return {"sp": pos}

    def rcopy(src, dst, ssem, rsem, dev):
        return pltpu.make_async_remote_copy(
            src_ref=src,
            dst_ref=dst,
            send_sem=ssem,
            recv_sem=rsem,
            device_id=dev,
            device_id_type=pl.DeviceIdType.MESH,
        )

    def signal(sem, dev):
        pl.semaphore_signal(sem, inc=1, device_id=dev, device_id_type=pl.DeviceIdType.MESH)

    moves = [
        (k_hbm, k_v),
        (v_hbm, v_v),
        (q_hbm, q_v),
        (sink_hbm, sink_s),
        (routes_hbm, routes_v),
        (gw_hbm, gw_v),
        (wo_hbm, wo_v),
        (res_hbm, res_v),
        (gain_hbm, gain_v),
        (sg_hbm, sg_v),
        (su_hbm, su_v),
        (sd_hbm, sd_v),
        (eg_hbm.at[0], eg_v),
        (eu_hbm.at[0], eu_v),
        (ed_hbm.at[0], ed_v),
    ]
    early = 9
    loads = [
        pltpu.make_async_copy(a, b, load_sem.at[i if i < early else i - early])
        for i, (a, b) in enumerate(moves)
    ]
    pending = []

    def sent(copy, condition=None):
        pending.append((copy, condition))

    def slot():
        if len(pending) >= SENDS:
            settle(pending[len(pending) - SENDS])
        return send_sem.at[len(pending) % SENDS]

    def settle(entry):
        copy, condition = entry
        if condition is None:
            copy.wait_send()
        else:
            pl.when(condition)(copy.wait_send)

    barrier = pltpu.get_barrier_semaphore()
    for dev in (core, xnbr):
        signal(barrier, dev)

    @pl.when(z > 0)
    def _():
        signal(barrier, at_z(z - 1))

    @pl.when(z < sp - 1)
    def _():
        signal(barrier, at_z(z + 1))

    for load in loads[:early]:
        load.start()
    rows = stream_v.shape[0]
    width = stream_v.shape[1]
    length = q_v.shape[0]
    heads = q_v.shape[1] // HEAD
    kv_heads = k_v.shape[1] // HEAD
    grouped = heads // kv_heads

    @pl.when(z == 0)
    def _():
        halo_k[0] = jnp.zeros(halo_k.shape[1:], halo_k.dtype)
        halo_v[0] = jnp.zeros(halo_v.shape[1:], halo_v.dtype)

    @pl.when(z == sp - 1)
    def _():
        halo_k[1] = jnp.zeros(halo_k.shape[1:], halo_k.dtype)
        halo_v[1] = jnp.zeros(halo_v.shape[1:], halo_v.dtype)

    loads[0].wait()
    loads[1].wait()
    peers = 2 + jnp.where(z > 0, 1, 0) + jnp.where(z < sp - 1, 1, 0)
    pl.semaphore_wait(barrier, peers)

    def halo(up, which, sem):
        pos = z + 1 if up else z - 1
        row = 0 if up else 1
        src = (k_v, v_v)[which]
        dst = (halo_k, halo_v)[which]
        return rcopy(src, dst.at[row], sem, halo_r.at[row, which], at_z(pos))

    def halo_wait(row, which):
        src = (k_v, v_v)[which]
        dst = (halo_k, halo_v)[which]
        rcopy(src, dst.at[row], send_sem.at[0], halo_r.at[row, which], core).wait_recv()

    for which in range(2):
        for up, condition in ((True, z < sp - 1), (False, z > 0)):
            copy = halo(up, which, slot())
            pl.when(condition)(copy.start)
            sent(copy, condition)

    def push(i, src, dst):
        return rcopy(src, dst, w_s.at[i], w_r.at[i], core)

    pushes = [
        push(0, eg_hbm.at[0], eg_o),
        push(1, sg_hbm, sg_o),
        push(2, su_hbm, su_o),
        push(3, sd_hbm, sd_o),
        push(4, eu_hbm.at[0], eu_o),
        push(5, ed_hbm.at[0], ed_o),
    ]
    for copy in pushes[:2]:
        copy.start()

    for k in range(2, 6):
        loads[k].wait()
    for load in loads[early:]:
        load.start()
    half = LANES // 2
    lane = lax.broadcasted_iota(jnp.int32, (rows, LANES), 1)
    unit = lax.broadcasted_iota(jnp.int32, (LANES, rows), 0)
    unit = jnp.where(unit < half, unit, unit - half)
    combine = jnp.zeros((LANES, rows), jnp.float32)
    for k in range(TOPK):
        combine = combine + jnp.where(routes_v[k : k + 1] == unit, gw_v[k : k + 1], 0.0)
    combine = combine.T
    high = combine.astype(jnp.bfloat16)
    low = (combine - high.astype(jnp.float32)).astype(jnp.bfloat16)
    own_tail = jnp.where(
        lane < half, high.astype(jnp.float32), low.astype(jnp.float32)
    ).astype(jnp.bfloat16)
    nrm[z, x, :, width:] = own_tail
    tail_s[...] = own_tail
    tail_copy = rcopy(tail_s, tail_m, slot(), w_r.at[6], xnbr)
    tail_copy.start()
    sent(tail_copy)

    contract = (((1,), (1,)), ((), ()))
    scale = HEAD ** (-0.5)

    def cols(head):
        return slice(head * HEAD, (head + 1) * HEAD)

    def stacked(kv):
        first = kv * grouped
        return jnp.concatenate(
            [q_v[:, cols(first + i)] for i in range(grouped)], axis=0
        ) * jnp.asarray(scale, q_v.dtype)

    def product(a, b):
        return lax.dot_general(a, b, contract, preferred_element_type=jnp.float32)

    queries = [stacked(kv) for kv in range(kv_heads)]
    row = lax.broadcasted_iota(jnp.int32, (grouped * length, 1), 0)
    tops = []
    sums = []
    outs = []
    for kv in range(kv_heads):
        scores = product(queries[kv], k_v[:, cols(kv)])
        sink = jnp.full((grouped * length, 1), sink_s[kv * grouped], jnp.float32)
        for i in range(1, grouped):
            sink = jnp.where(row >= i * length, sink_s[kv * grouped + i], sink)
        top = jnp.maximum(jnp.max(scores, axis=-1, keepdims=True), sink)
        e = jnp.exp(scores - top)
        tops.append(top)
        sums.append(jnp.exp(sink - top) + jnp.sum(e, axis=-1, keepdims=True))
        outs.append(
            jnp.dot(e.astype(jnp.bfloat16), v_v[:, cols(kv)], preferred_element_type=jnp.float32)
        )

    qi = lax.broadcasted_iota(jnp.int32, (grouped * length, length), 0) % length
    ki = lax.broadcasted_iota(jnp.int32, (grouped * length, length), 1)
    low_bound = jnp.where(z > 0, 0, length)
    high_bound = jnp.where(z < sp - 1, 0, length)
    low_mask = ki - qi >= low_bound
    high_mask = qi - ki >= high_bound

    def wait_halo(which):
        @pl.when(z > 0)
        def _():
            halo_wait(0, which)

        @pl.when(z < sp - 1)
        def _():
            halo_wait(1, which)

    wait_halo(0)
    sides = []
    for kv in range(kv_heads):
        s_low = jnp.where(low_mask, product(queries[kv], halo_k[0, :, cols(kv)]), -jnp.inf)
        s_high = jnp.where(high_mask, product(queries[kv], halo_k[1, :, cols(kv)]), -jnp.inf)
        top = jnp.max(jnp.maximum(s_low, s_high), axis=-1, keepdims=True)
        top = jnp.maximum(top, tops[kv])
        e_low = jnp.exp(s_low - top)
        e_high = jnp.exp(s_high - top)
        shrink = jnp.exp(tops[kv] - top)
        denominator = shrink * sums[kv] + jnp.sum(e_low + e_high, axis=-1, keepdims=True)
        sides.append(
            (
                shrink * outs[kv],
                e_low.astype(jnp.bfloat16),
                e_high.astype(jnp.bfloat16),
                1.0 / denominator,
            )
        )
    wait_halo(1)
    for kv in range(kv_heads):
        base, e_low, e_high, inverse = sides[kv]
        base = base + jnp.dot(
            e_low, halo_v[0, :, cols(kv)], preferred_element_type=jnp.float32
        )
        base = base + jnp.dot(
            e_high, halo_v[1, :, cols(kv)], preferred_element_type=jnp.float32
        )
        base = (base * inverse).astype(jnp.bfloat16)
        for i in range(grouped):
            att_v[:, :, cols(kv * grouped + i)] = base[i * length : (i + 1) * length].reshape(
                tp, rows, HEAD
            )

    @pl.when(z == 1)
    def _():
        signal(far_sem, at_z(z - 1))

    @pl.when(z == sp - 2)
    def _():
        signal(far_sem, at_z(z + 1))

    loads[6].wait()

    def projected(cc):
        picked = jnp.concatenate([att_v[xh * PAIR + cc] for xh in range(PAIR)], axis=0)
        return jnp.dot(picked, wo_v[...], preferred_element_type=jnp.float32)

    psend[...] = projected(1 - c).astype(jnp.bfloat16).reshape(psend.shape)
    pcore = []
    for order, xx in enumerate((1 - x, x)):
        pcore.append(rcopy(psend.at[xx], precv.at[xx], slot(), pr_sem.at[order], core))
        pcore[-1].start()
        sent(pcore[-1])
    for copy in pushes[2:]:
        copy.start()
    proj[...] = projected(c).reshape(proj.shape)
    piece = rows // CHUNKS

    def cut(j):
        return pl.ds(j * piece, piece)

    def cross(src, dst, k):
        copy = rcopy(src, dst, slot(), pr_sem.at[PAIR + k], xnbr)
        copy.start()
        sent(copy)
        return copy

    pcore[0].wait_recv()
    mirror_v[...] = proj[1 - x] + precv[1 - x].astype(jnp.float32)
    pcross = []
    for j in range(CHUNKS):
        pxs[cut(j)] = mirror_v[cut(j)].astype(jnp.bfloat16)
        pcross.append(cross(pxs.at[cut(j)], pxr.at[cut(j)], j))
    loads[7].wait()
    loads[8].wait()
    pcore[1].wait_recv()
    stream_v[...] = res_v[...].astype(jnp.float32) + proj[x] + precv[x].astype(jnp.float32)
    pmirror = []
    for j in range(CHUNKS):
        pys[cut(j)] = stream_v[cut(j)].astype(jnp.bfloat16)
        pmirror.append(cross(pys.at[cut(j)], pyr.at[cut(j)], CHUNKS + j))
    tail_copy.wait_recv()
    nrm[z, 1 - x, :, width:] = tail_m[...]

    def normalized(stream):
        return (
            stream
            * lax.rsqrt(jnp.mean(stream * stream, axis=-1, keepdims=True) + norm_eps)
            * gain_v[...]
        ).astype(jnp.bfloat16)

    expert = z * tp + t
    sibling = z * tp + t_core

    def schedule(me):
        def place(p):
            return p + upper * (sp - 1 - 2 * p)

        def send(src, dst, rsem, dev):
            copy = rcopy(src, dst, slot(), rsem, dev)
            copy.start()
            sent(copy)

        def side(h):
            return x if h == "o" else 1 - x

        def block_send(p, h, j, dev):
            g = place(p)
            ref = nrm.at[g, side(h), cut(j)]
            send(ref, ref, nrm_r.at[g, side(h), j], dev)

        def block_wait(p, h, j):
            g = place(p)
            ref = nrm.at[g, side(h), cut(j)]
            rcopy(ref, ref, send_sem.at[0], nrm_r.at[g, side(h), j], core).wait_recv()

        def cross_copy(p, j, sem):
            g = place(p)
            return rcopy(
                xsend.at[g, cut(j)], xrecv.at[g, cut(j)], sem, xr_sem.at[g, j], xnbr
            )

        lane_of = {"o": 0, "m": 1}

        def line_send(p, h, span):
            g = place(p)
            send(
                zsend.at[g, side(h), span],
                zrecv.at[z, side(h), span],
                zr_sem.at[z, lane_of[h]],
                at_z(g),
            )

        def line_wait(p, h):
            g = place(p)
            ref = zrecv.at[g, side(h)]
            rcopy(ref, ref, send_sem.at[0], zr_sem.at[g, lane_of[h]], core).wait_recv()
            return zrecv[g, side(h)].astype(jnp.float32)

        def add_send(p, j, adder):
            g = place(p)
            send(
                zsend.at[g, x, cut(j)], zadd.at[g, cut(j)], za_sem.at[g, j], at_z(place(adder))
            )

        def add_wait(p, j):
            g = place(p)
            ref = zadd.at[g, cut(j)]
            rcopy(ref, ref, send_sem.at[0], za_sem.at[g, j], core).wait_recv()
            return zadd[g, cut(j)].astype(jnp.float32)

        def cross_wait(p, j):
            cross_copy(p, j, send_sem.at[0]).wait_recv()
            g = place(p)
            return part[g, x, cut(j)] + xrecv[g, cut(j)].astype(jnp.float32)

        waited = set()

        def once(name, copies):
            if name not in waited:
                waited.add(name)
                for copy in copies:
                    copy()

        def own_weights():
            once("own", [loads[k].wait for k in range(9, 15)])

        def sibling_experts():
            once("experts", [pushes[k].wait_recv for k in (0, 4, 5)])

        def sibling_shared():
            once("shared", [pushes[k].wait_recv for k in (1, 2, 3)])

        def one(acts, gate_ref, up_ref, down_ref):
            gate = jnp.dot(acts, gate_ref[...], preferred_element_type=jnp.float32)
            up = jnp.dot(acts, up_ref[...], preferred_element_type=jnp.float32)
            hidden = (silu(gate) * up).astype(jnp.bfloat16)
            out = jnp.dot(hidden, down_ref[...], preferred_element_type=jnp.float32)
            return out.astype(jnp.bfloat16).astype(jnp.float32)

        def rows_of(places):
            block = [nrm[g].reshape(PAIR * rows, nrm.shape[-1]) for g in places]
            block = jnp.concatenate(block * 2 if len(block) == 1 else block, axis=0)
            return block[:, :width], block[:, width:].astype(jnp.float32)

        def weight(tail, e):
            lanes = lax.broadcasted_iota(jnp.int32, tail.shape, 1)
            mine = (lanes == e) | (lanes == e + half)
            return jnp.sum(jnp.where(mine, tail, 0.0), axis=-1, keepdims=True)

        def experts(ps):
            own_weights()
            sibling_experts()
            places = [place(p) for p in ps]
            acts, tail = rows_of(places)
            result = weight(tail, expert) * one(acts, eg_v, eu_v, ed_v)
            result = result + weight(tail, sibling) * one(acts, eg_o, eu_o, ed_o)
            result = result[: len(ps) * PAIR * rows].reshape(len(ps), PAIR, rows, width)
            for i, g in enumerate(places):
                part[g] = result[i]

        own_parts = [op for op in ORDER[me] if op[0] == "Q"]

        def own_part(op):
            own_weights()
            acts, tail = rows_of([z])
            if op[1] == 0:
                result = weight(tail, expert) * one(acts, eg_v, eu_v, ed_v)
            elif op[1] == 1:
                sibling_experts()
                result = weight(tail, sibling) * one(acts, eg_o, eu_o, ed_o)
            else:
                sibling_shared()
                result = one(acts, sg_v, su_v, sd_v) + one(acts, sg_o, su_o, sd_o)
            result = result[: PAIR * rows].reshape(PAIR, rows, width)
            if op == own_parts[0]:
                part[z] = result
            else:
                part[z] = part[z] + result

        knows_far = False
        summed = set()
        tail_from = None
        for op in ORDER[me]:
            kind = op[0]
            if kind == "E" and tail_from is None:
                tail_from = len(pending)
            if kind in "HG" and not summed:
                for entry in pending[max(0, len(pending) - SENDS) : tail_from]:
                    settle(entry)
                for copy in pushes:
                    copy.wait_send()
                settled = max(tail_from, len(pending) - SENDS)
                summed.add(me)
            with jax.named_scope("op_" + "_".join(str(v) for v in op)):
                if kind == "N":
                    j = op[1]
                    pcross[j].wait_recv()
                    stream = stream_v[cut(j)] + pxr[cut(j)].astype(jnp.float32)
                    stream_v[cut(j)] = stream
                    nrm[z, x, cut(j), :width] = normalized(stream)
                elif kind == "M":
                    j = op[1]
                    pmirror[j].wait_recv()
                    stream = mirror_v[cut(j)] + pyr[cut(j)].astype(jnp.float32)
                    nrm[z, 1 - x, cut(j), :width] = normalized(stream)
                elif kind == "S":
                    h, p, j = op[1:]
                    if relay_of(me, p) is None and (
                        h == "o" or listed(me, p, DISPATCH_BY_LINE)
                    ):
                        if me == 0 and p == LINE - 1 and not knows_far:
                            pl.semaphore_wait(far_sem, 1)
                            knows_far = True
                        block_send(me, h, j, at_z(place(p)))
                elif kind == "A":
                    p, h, j = op[1:]
                    block_wait(p, h, j)
                    mirrored_in = listed(p, me, DISPATCH_BY_LINE)
                    if h == "o" and not mirrored_in:
                        block_send(p, h, j, xnbr)
                    for q in range(LINE):
                        if q not in (p, me) and relay_of(p, q) == me:
                            if h == "o" or (mirrored_in and listed(p, q, DISPATCH_BY_LINE)):
                                block_send(p, h, j, at_z(place(q)))
                elif kind == "D":
                    experts(op[1])
                elif kind == "Q":
                    own_part(op)
                elif kind == "E":
                    p = op[1]
                    g = place(p)
                    if p != me and listed(me, p, RETURN_BY_LINE):
                        for h in ("o", "m"):
                            zsend[g, side(h)] = part[g, side(h)].astype(jnp.bfloat16)
                            line_send(p, h, slice(None))
                    else:
                        if p == me:
                            for q in range(LINE):
                                if q != me and listed(q, me, RETURN_BY_LINE):
                                    part[g, 1 - x] = part[g, 1 - x] + line_wait(q, "m")
                        for j in range(CHUNKS):
                            xsend[g, cut(j)] = part[g, 1 - x, cut(j)].astype(jnp.bfloat16)
                            copy = cross_copy(p, j, slot())
                            copy.start()
                            sent(copy)
                elif kind == "F":
                    p, j = op[1:]
                    if not listed(me, p, RETURN_BY_LINE):
                        value = cross_wait(p, j)
                        for q in range(LINE):
                            if q not in (p, me) and adder_of(q, p) == me:
                                value = value + add_wait(p, j)
                        zsend[place(p), x, cut(j)] = value.astype(jnp.bfloat16)
                        adder = adder_of(me, p)
                        if adder is None:
                            line_send(p, "o", cut(j))
                        else:
                            add_send(p, j, adder)
                elif kind == "H":
                    j = op[1]
                    stream_v[cut(j)] = stream_v[cut(j)] + cross_wait(me, j)
                elif kind == "G":
                    p = op[1]
                    if p not in summed and adder_of(p, me) is None:
                        stream_v[...] = stream_v[...] + line_wait(p, "o")
                    summed.add(p)
        out_ref[...] = stream_v[...].astype(out_ref.dtype)
        if me == 0 and not knows_far:
            pl.semaphore_wait(far_sem, 1)
        with jax.named_scope("lastwaits"):
            for entry in pending[settled:]:
                settle(entry)

    shared_pending = list(pending)
    for me in range(LINE // 2):

        @pl.when((z == me) | (z == sp - 1 - me))
        def _():
            pending[:] = shared_pending
            schedule(me)


def fused_scratch(sp, tp, shapes):
    (q, k, v, sink, wo, res, gain, routes, gw, eg, eu, ed, sg, su, sd) = shapes
    rows, width = res.shape
    bf = jnp.bfloat16
    f32 = jnp.float32
    return [
        (q.shape, bf),
        (k.shape, bf),
        (v.shape, bf),
        (sink.shape, f32),
        (wo.shape, bf),
        (res.shape, bf),
        (gain.shape, f32),
        (routes.shape, jnp.int32),
        (gw.shape, f32),
        (eg.shape[1:], bf),
        (eu.shape[1:], bf),
        (ed.shape[1:], bf),
        (sg.shape, bf),
        (su.shape, bf),
        (sd.shape, bf),
        (eg.shape[1:], bf),
        (eu.shape[1:], bf),
        (ed.shape[1:], bf),
        (sg.shape, bf),
        (su.shape, bf),
        (sd.shape, bf),
        ((2,) + k.shape, bf),
        ((2,) + v.shape, bf),
        ((tp, rows, q.shape[1]), bf),
        ((PAIR, rows, width), f32),
        ((PAIR, rows, width), bf),
        ((PAIR, rows, width), bf),
        ((rows, width), bf),
        ((rows, width), bf),
        ((rows, width), bf),
        ((rows, width), bf),
        ((rows, width), f32),
        ((rows, width), f32),
        ((rows, LANES), bf),
        ((rows, LANES), bf),
        ((sp, PAIR, rows, width + LANES), bf),
        ((sp, PAIR, rows, width), f32),
        ((sp, rows, width), bf),
        ((sp, rows, width), bf),
        ((sp, PAIR, rows, width), bf),
        ((sp, PAIR, rows, width), bf),
        ((sp, rows, width), bf),
    ]


def size_of(shape, dtype):
    total = jnp.dtype(dtype).itemsize
    for extent in shape:
        total *= extent
    return total


def fused(sp, tp, buffers, *args):
    dma = pltpu.SemaphoreType.DMA
    res = args[5]
    scratch = [pltpu.VMEM(s, d) for s, d in buffers]
    scratch[3] = pltpu.SMEM(*buffers[3])
    return pl.pallas_call(
        functools.partial(fused_kernel, sp, tp),
        out_shape=pltpu.VMEM(res.shape, jnp.bfloat16),
        in_specs=[pl.BlockSpec(memory_space=pltpu.HBM)] * 15,
        out_specs=pl.BlockSpec(memory_space=pltpu.VMEM),
        scratch_shapes=scratch
        + [
            dma((9,)),
            dma((2, 2)),
            dma((PAIR + 2 * CHUNKS,)),
            dma((6,)),
            dma((7,)),
            dma((SENDS,)),
            dma((sp, PAIR, CHUNKS)),
            dma((sp, CHUNKS)),
            dma((sp, PAIR)),
            dma((sp, CHUNKS)),
            pltpu.SemaphoreType.REGULAR,
        ],
        compiler_params=pltpu.CompilerParams(
            collective_id=0, has_side_effects=True, vmem_limit_bytes=VMEM_BYTES
        ),
    )(*args)


def either(*args):
    sp = lax.axis_size("sp")
    tp = lax.axis_size("tp")
    args = list(args)
    shaped = list(args)
    shaped[6] = args[6].reshape(1, -1)
    shaped[7] = args[7].T
    shaped[8] = args[8].T
    buffers = fused_scratch(sp, tp, shaped)
    needed = sum(size_of(s, d) for s, d in buffers)
    fits = (
        2 * needed <= VMEM_BYTES
        and tp == 2 * PAIR
        and sp == LINE
        and args[5].shape[0] % (16 * CHUNKS) == 0
        and 2 * sp * tp <= LANES
        and args[0].shape[0] == WINDOW
        and args[9].shape[0] == 1
    )
    if fits:
        return fused(sp, tp, buffers, *shaped)
    return body(*args)


def solution(mesh):
    placed = (
        P(("grp", "sp"), "tp"),
        P(("grp", "sp"), "tp"),
        P(("grp", "sp"), "tp"),
        P("tp"),
        P("tp", None),
        P(("grp", "sp", "tp"), None),
        P(),
        P(("grp", "sp", "tp"), None),
        P(("grp", "sp", "tp"), None),
        P(("sp", "tp"), None, None),
        P(("sp", "tp"), None, None),
        P(("sp", "tp"), None, None),
        P(None, "tp"),
        P(None, "tp"),
        P("tp", None),
    )
    return jax.shard_map(
        either, mesh=mesh, in_specs=placed, out_specs=P(("grp", "sp", "tp"), None), check_vma=False
    )
```

time: 48.4 us -> 47.6 us (0.983)
  Pallas kernels: 47.6 us -> 46.8 us
    pallas_call x1, Pallas kernels: 47.6 us -> 46.8 us  [fused(): pl.pallas_call(functools.partial(fused_kernel, sp, tp), out_shape=pltpu.V...]
where the time goes in v2:
time: 47.6 us; the launch traced here: 47.5 us
  Pallas kernels  46.8 us (98%)
  local copies, waits for them, and re-layouts  0.66 us (1%)
    pallas_call x1, Pallas kernels, fused(): pl.pallas_call(functools.partial(fused_kernel, sp, tp), out_shape=pltpu.V...  46.8 us

profile of v2, /device:TPU:0, one launch (start us, length us, event | category | flops | bytes accessed | tf_op | source)
XLA Modules:
  0.0 47.5 jit_solution(7626273119226614983)
XLA Ops:
  0.0 46.8 %shard_map.145 = bf16[32,2048]{1,0:T(8,128)(2,1)S(1)} custom-call(bf16[128,256]{1,0:T(8,128)(2,1)} %q_hbm.1, bf16[128,128]{1,0:T(8,128)(2,1)} %k_hbm.1, bf16[128,128]{1,0:T(8,128)(2,1)} %v_hbm.1, f32[4]{0:T(128)} %sink_hbm.1, bf16[256,2048]{1,0:T(8,128)(2,1)} %wo_hbm.1, bf16[32,2048]{1,0:T(8,128)(2,1)} %res_hbm.1, f32[1,2048]{1,0:T(1,128)} %bitcast.3, ...), custom_call_target="tpu_custom_call" | custom-call | tf_op jit(solution)/shard_map/pallas_call | solution.py:957
  46.8 0.7 %copy.17 = bf16[32,2048]{1,0:T(8,128)(2,1)} copy(bf16[32,2048]{1,0:T(8,128)(2,1)S(1)} %shard_map.145) | data formatting | bytes 262144

commit v3 on v2

--- a/solution.py
+++ b/solution.py
@@ -145,115 +145,117 @@
 LANES = 128
 CHUNKS = 2
 SENDS = 20
-DISPATCH_BY_LINE = ((0, 1),)
-RETURN_BY_LINE = ((0, 2), (1, 0),)
-RELAYS = {(0, 3): 2, (1, 3): 2}
-ADDERS = {}
+DISPATCH_BY_LINE = ()
+RETURN_BY_LINE = ((0, 1), (1, 3),)
+RELAYS = {(0, 2): 1, (0, 3): 2, (1, 3): 2}
+ADDERS = {(0, 2): 1, (0, 3): 1}
 ORDER = {
     0: (
+        ("N", 1),
         ("N", 0),
+        ("S", "o", 1, 1),
+        ("A", 1, "o", 0),
         ("S", "o", 1, 0),
-        ("N", 1),
+        ("A", 1, "o", 1),
+        ("A", 1, "m", 0),
+        ("A", 1, "m", 1),
+        ("A", 2, "o", 0),
+        ("A", 2, "o", 1),
+        ("D", (1,)),
         ("M", 0),
-        ("S", "o", 2, 0),
-        ("A", 1, "o", 0),
         ("M", 1),
-        ("S", "o", 3, 0),
-        ("S", "o", 2, 1),
-        ("S", "m", 2, 0),
-        ("S", "o", 3, 1),
-        ("Q", 0),
-        ("A", 1, "o", 1),
-        ("S", "m", 1, 0),
-        ("S", "m", 1, 1),
-        ("S", "m", 2, 1),
-        ("A", 2, "o", 0),
-        ("Q", 2),
-        ("A", 2, "o", 1),
-        ("S", "o", 1, 1),
+        ("E", 1),
+        ("A", 2, "m", 0),
         ("A", 3, "o", 0),
+        ("F", 1, 0),
         ("A", 3, "o", 1),
         ("A", 2, "m", 1),
-        ("A", 1, "m", 0),
-        ("A", 1, "m", 1),
-        ("A", 2, "m", 0),
+        ("D", (2,)),
+        ("E", 2),
+        ("S", "o", 2, 1),
+        ("A", 3, "m", 0),
+        ("S", "m", 1, 0),
+        ("A", 3, "m", 1),
+        ("S", "m", 2, 1),
+        ("S", "o", 3, 1),
+        ("D", (3,)),
+        ("F", 2, 0),
+        ("E", 3),
+        ("Q", 1),
+        ("F", 2, 1),
+        ("Q", 0),
+        ("F", 3, 0),
         ("S", "m", 3, 1),
-        ("D", (1, 2)),
-        ("E", 2),
-        ("A", 3, "m", 1),
-        ("A", 3, "m", 0),
-        ("E", 1),
-        ("D", (3,)),
-        ("E", 3),
+        ("Q", 2),
+        ("F", 1, 1),
+        ("S", "m", 2, 0),
+        ("G", 2, 1),
+        ("F", 3, 1),
+        ("E", 0),
+        ("G", 1, 0),
+        ("S", "m", 1, 1),
+        ("H", 0),
         ("S", "m", 3, 0),
-        ("F", 3, 0),
-        ("F", 3, 1),
-        ("F", 1, 1),
-        ("F", 1, 0),
-        ("Q", 1),
-        ("E", 0),
-        ("F", 2, 1),
-        ("G", 2, 1),
+        ("G", 2, 0),
+        ("G", 3, 0),
+        ("S", "o", 3, 0),
+        ("G", 3, 1),
         ("H", 1),
-        ("G", 3, 0),
         ("G", 1, 1),
-        ("F", 2, 0),
-        ("G", 1, 0),
-        ("H", 0),
-        ("G", 2, 0),
-        ("G", 3, 1),
+        ("S", "o", 2, 0),
     ),
     1: (
         ("N", 0),
+        ("S", "o", 0, 0),
         ("S", "o", 2, 0),
-        ("S", "o", 0, 0),
         ("N", 1),
+        ("M", 0),
         ("S", "o", 0, 1),
-        ("S", "o", 3, 0),
         ("S", "o", 2, 1),
-        ("M", 0),
+        ("A", 2, "o", 0),
+        ("S", "o", 3, 1),
         ("M", 1),
+        ("A", 0, "o", 1),
+        ("S", "m", 3, 1),
+        ("S", "m", 2, 1),
+        ("A", 2, "o", 1),
         ("A", 0, "o", 0),
-        ("A", 2, "o", 0),
-        ("S", "m", 2, 0),
-        ("Q", 0),
-        ("A", 2, "o", 1),
+        ("Q", 2),
         ("A", 3, "o", 0),
         ("A", 3, "o", 1),
+        ("A", 3, "m", 1),
+        ("A", 2, "m", 0),
+        ("A", 3, "m", 0),
+        ("D", (3,)),
+        ("S", "m", 0, 1),
+        ("A", 0, "m", 1),
+        ("E", 3),
+        ("A", 0, "m", 0),
         ("A", 2, "m", 1),
-        ("A", 0, "o", 1),
-        ("A", 3, "m", 1),
-        ("A", 0, "m", 0),
-        ("A", 3, "m", 0),
-        ("A", 2, "m", 0),
-        ("A", 0, "m", 1),
-        ("D", (0, 2, 3)),
+        ("S", "m", 2, 0),
+        ("S", "o", 3, 0),
+        ("D", (0, 2)),
+        ("E", 0),
+        ("Q", 1),
+        ("G", 3, 1),
         ("E", 2),
-        ("E", 0),
-        ("Q", 2),
-        ("S", "m", 3, 1),
-        ("Q", 1),
-        ("S", "m", 0, 1),
-        ("S", "o", 3, 1),
+        ("Q", 0),
         ("F", 2, 0),
-        ("E", 3),
         ("F", 0, 0),
+        ("E", 1),
         ("F", 3, 1),
-        ("S", "m", 2, 1),
-        ("F", 3, 0),
+        ("F", 0, 1),
+        ("F", 2, 1),
+        ("G", 0, 0),
+        ("H", 1),
+        ("H", 0),
+        ("G", 2, 0),
         ("S", "m", 0, 0),
-        ("S", "m", 3, 0),
-        ("E", 1),
-        ("F", 2, 1),
-        ("H", 0),
-        ("H", 1),
         ("G", 0, 1),
         ("G", 3, 0),
-        ("F", 0, 1),
-        ("G", 2, 0),
+        ("F", 3, 0),
         ("G", 2, 1),
-        ("G", 3, 1),
-        ("G", 0, 0),
+        ("S", "m", 3, 0),
     ),
 }
 
@@ -417,11 +419,14 @@
 
     def slot():
         if len(pending) >= SENDS:
-            settle(pending[len(pending) - SENDS])
+            settle(len(pending) - SENDS)
         return send_sem.at[len(pending) % SENDS]
 
-    def settle(entry):
-        copy, condition = entry
+    def settle(index):
+        copy, condition = pending[index]
+        if copy is None:
+            return
+        pending[index] = (None, None)
         if condition is None:
             copy.wait_send()
         else:
@@ -796,11 +801,10 @@
             if kind == "E" and tail_from is None:
                 tail_from = len(pending)
             if kind in "HG" and not summed:
-                for entry in pending[max(0, len(pending) - SENDS) : tail_from]:
-                    settle(entry)
+                for index in range(tail_from):
+                    settle(index)
                 for copy in pushes:
                     copy.wait_send()
-                settled = max(tail_from, len(pending) - SENDS)
                 summed.add(me)
             with jax.named_scope("op_" + "_".join(str(v) for v in op)):
                 if kind == "N":
@@ -872,15 +876,15 @@
                     stream_v[cut(j)] = stream_v[cut(j)] + cross_wait(me, j)
                 elif kind == "G":
                     p = op[1]
-                    if p not in summed and adder_of(p, me) is None:
+                    last = [other for other in ORDER[me] if other[:2] == ("G", p)][-1]
+                    if op == last and adder_of(p, me) is None:
                         stream_v[...] = stream_v[...] + line_wait(p, "o")
-                    summed.add(p)
         out_ref[...] = stream_v[...].astype(out_ref.dtype)
         if me == 0 and not knows_far:
             pl.semaphore_wait(far_sem, 1)
         with jax.named_scope("lastwaits"):
-            for entry in pending[settled:]:
-                settle(entry)
+            for index in range(len(pending)):
+                settle(index)
 
     shared_pending = list(pending)
     for me in range(LINE // 2):

time: 47.6 us -> 45 us (0.945)
  Pallas kernels: 46.8 us -> 44.2 us
    pallas_call x1, Pallas kernels: 46.8 us -> 44.2 us  [fused(): pl.pallas_call(functools.partial(fused_kernel, sp, tp), out_shape=pltpu.V...]
where the time goes in v3:
time: 45 us; the launch traced here: 44.9 us
  Pallas kernels  44.2 us (98%)
  local copies, waits for them, and re-layouts  0.66 us (1%)
    pallas_call x1, Pallas kernels, fused(): pl.pallas_call(functools.partial(fused_kernel, sp, tp), out_shape=pltpu.V...  44.2 us

profile of v3, /device:TPU:0, one launch (start us, length us, event | category | flops | bytes accessed | tf_op | source)
XLA Modules:
  0.0 44.9 jit_solution(5035267365984616761)
XLA Ops:
  0.0 44.2 %shard_map.145 = bf16[32,2048]{1,0:T(8,128)(2,1)S(1)} custom-call(bf16[128,256]{1,0:T(8,128)(2,1)} %q_hbm.1, bf16[128,128]{1,0:T(8,128)(2,1)} %k_hbm.1, bf16[128,128]{1,0:T(8,128)(2,1)} %v_hbm.1, f32[4]{0:T(128)} %sink_hbm.1, bf16[256,2048]{1,0:T(8,128)(2,1)} %wo_hbm.1, bf16[32,2048]{1,0:T(8,128)(2,1)} %res_hbm.1, f32[1,2048]{1,0:T(1,128)} %bitcast.3, ...), custom_call_target="tpu_custom_call" | custom-call | tf_op jit(solution)/shard_map/pallas_call | solution.py:961
  44.2 0.7 %copy.17 = bf16[32,2048]{1,0:T(8,128)(2,1)} copy(bf16[32,2048]{1,0:T(8,128)(2,1)S(1)} %shard_map.145) | data formatting | bytes 262144

commit v4 on v3

--- a/solution.py
+++ b/solution.py
@@ -145,117 +145,117 @@
 LANES = 128
 CHUNKS = 2
 SENDS = 20
-DISPATCH_BY_LINE = ()
+DISPATCH_BY_LINE = ((1, 2),)
 RETURN_BY_LINE = ((0, 1), (1, 3),)
 RELAYS = {(0, 2): 1, (0, 3): 2, (1, 3): 2}
-ADDERS = {(0, 2): 1, (0, 3): 1}
+ADDERS = {(0, 2): 1, (1, 3): 2}
 ORDER = {
     0: (
+        ("N", 0),
+        ("S", "o", 1, 0),
         ("N", 1),
-        ("N", 0),
         ("S", "o", 1, 1),
         ("A", 1, "o", 0),
-        ("S", "o", 1, 0),
+        ("M", 0),
+        ("S", "o", 2, 0),
         ("A", 1, "o", 1),
+        ("M", 1),
+        ("Q", 2),
+        ("Q", 1),
+        ("A", 2, "o", 0),
+        ("S", "m", 2, 1),
         ("A", 1, "m", 0),
+        ("A", 2, "o", 1),
         ("A", 1, "m", 1),
-        ("A", 2, "o", 0),
-        ("A", 2, "o", 1),
         ("D", (1,)),
-        ("M", 0),
-        ("M", 1),
+        ("A", 3, "o", 0),
+        ("A", 2, "m", 0),
+        ("A", 3, "o", 1),
         ("E", 1),
-        ("A", 2, "m", 0),
-        ("A", 3, "o", 0),
-        ("F", 1, 0),
-        ("A", 3, "o", 1),
         ("A", 2, "m", 1),
         ("D", (2,)),
         ("E", 2),
+        ("S", "o", 3, 0),
+        ("A", 3, "m", 0),
+        ("A", 3, "m", 1),
+        ("F", 1, 1),
+        ("D", (3,)),
         ("S", "o", 2, 1),
-        ("A", 3, "m", 0),
+        ("E", 3),
+        ("F", 2, 1),
+        ("S", "m", 3, 1),
+        ("F", 2, 0),
+        ("Q", 0),
+        ("S", "o", 3, 1),
+        ("G", 2, 0),
+        ("F", 3, 0),
         ("S", "m", 1, 0),
-        ("A", 3, "m", 1),
-        ("S", "m", 2, 1),
-        ("S", "o", 3, 1),
-        ("D", (3,)),
-        ("F", 2, 0),
-        ("E", 3),
-        ("Q", 1),
-        ("F", 2, 1),
-        ("Q", 0),
-        ("F", 3, 0),
-        ("S", "m", 3, 1),
-        ("Q", 2),
-        ("F", 1, 1),
+        ("F", 3, 1),
+        ("F", 1, 0),
+        ("E", 0),
+        ("H", 0),
+        ("G", 3, 0),
+        ("S", "m", 1, 1),
+        ("G", 2, 1),
+        ("H", 1),
+        ("G", 1, 0),
         ("S", "m", 2, 0),
-        ("G", 2, 1),
-        ("F", 3, 1),
-        ("E", 0),
-        ("G", 1, 0),
-        ("S", "m", 1, 1),
-        ("H", 0),
+        ("G", 1, 1),
+        ("G", 3, 1),
         ("S", "m", 3, 0),
-        ("G", 2, 0),
-        ("G", 3, 0),
-        ("S", "o", 3, 0),
-        ("G", 3, 1),
-        ("H", 1),
-        ("G", 1, 1),
-        ("S", "o", 2, 0),
     ),
     1: (
         ("N", 0),
+        ("S", "o", 2, 0),
         ("S", "o", 0, 0),
-        ("S", "o", 2, 0),
         ("N", 1),
+        ("S", "o", 2, 1),
+        ("S", "o", 0, 1),
         ("M", 0),
-        ("S", "o", 0, 1),
-        ("S", "o", 2, 1),
+        ("A", 0, "o", 0),
         ("A", 2, "o", 0),
-        ("S", "o", 3, 1),
         ("M", 1),
         ("A", 0, "o", 1),
+        ("G", 3, 0),
+        ("A", 2, "o", 1),
+        ("A", 3, "o", 0),
+        ("S", "m", 2, 1),
+        ("Q", 1),
+        ("A", 0, "m", 1),
+        ("A", 3, "o", 1),
+        ("A", 2, "m", 1),
+        ("Q", 2),
+        ("A", 0, "m", 0),
+        ("S", "o", 3, 1),
+        ("S", "m", 2, 0),
+        ("A", 3, "m", 0),
+        ("A", 3, "m", 1),
+        ("D", (3,)),
+        ("E", 3),
+        ("A", 2, "m", 0),
+        ("D", (0, 2)),
+        ("E", 2),
+        ("G", 3, 1),
+        ("Q", 0),
+        ("S", "m", 0, 1),
+        ("E", 0),
+        ("F", 2, 1),
+        ("F", 0, 0),
+        ("F", 3, 1),
+        ("G", 0, 0),
+        ("F", 0, 1),
+        ("S", "m", 3, 0),
+        ("F", 2, 0),
+        ("G", 0, 1),
+        ("S", "m", 0, 0),
+        ("E", 1),
+        ("S", "o", 3, 0),
+        ("F", 3, 0),
         ("S", "m", 3, 1),
-        ("S", "m", 2, 1),
-        ("A", 2, "o", 1),
-        ("A", 0, "o", 0),
-        ("Q", 2),
-        ("A", 3, "o", 0),
-        ("A", 3, "o", 1),
-        ("A", 3, "m", 1),
-        ("A", 2, "m", 0),
-        ("A", 3, "m", 0),
-        ("D", (3,)),
-        ("S", "m", 0, 1),
-        ("A", 0, "m", 1),
-        ("E", 3),
-        ("A", 0, "m", 0),
-        ("A", 2, "m", 1),
-        ("S", "m", 2, 0),
-        ("S", "o", 3, 0),
-        ("D", (0, 2)),
-        ("E", 0),
-        ("Q", 1),
-        ("G", 3, 1),
-        ("E", 2),
-        ("Q", 0),
-        ("F", 2, 0),
-        ("F", 0, 0),
-        ("E", 1),
-        ("F", 3, 1),
-        ("F", 0, 1),
-        ("F", 2, 1),
-        ("G", 0, 0),
+        ("G", 2, 0),
+        ("G", 2, 1),
+        ("H", 0),
         ("H", 1),
-        ("H", 0),
-        ("G", 2, 0),
-        ("S", "m", 0, 0),
-        ("G", 0, 1),
-        ("G", 3, 0),
-        ("F", 3, 0),
-        ("G", 2, 1),
-        ("S", "m", 3, 0),
     ),
 }
 
@@ -800,7 +800,7 @@
             kind = op[0]
             if kind == "E" and tail_from is None:
                 tail_from = len(pending)
-            if kind in "HG" and not summed:
+            if kind in "HG" and tail_from is not None and not summed:
                 for index in range(tail_from):
                     settle(index)
                 for copy in pushes:

time: 45 us -> 43 us (0.956)
  Pallas kernels: 44.2 us -> 42.2 us
    pallas_call x1, Pallas kernels: 44.2 us -> 42.2 us  [fused(): pl.pallas_call(functools.partial(fused_kernel, sp, tp), out_shape=pltpu.V...]
where the time goes in v4:
time: 43 us; the launch traced here: 42.9 us
  Pallas kernels  42.2 us (98%)
  local copies, waits for them, and re-layouts  0.66 us (2%)
    pallas_call x1, Pallas kernels, fused(): pl.pallas_call(functools.partial(fused_kernel, sp, tp), out_shape=pltpu.V...  42.2 us

profile of v4, /device:TPU:0, one launch (start us, length us, event | category | flops | bytes accessed | tf_op | source)
XLA Modules:
  0.0 42.9 jit_solution(7204987187592650234)
XLA Ops:
  0.0 42.2 %shard_map.145 = bf16[32,2048]{1,0:T(8,128)(2,1)S(1)} custom-call(bf16[128,256]{1,0:T(8,128)(2,1)} %q_hbm.1, bf16[128,128]{1,0:T(8,128)(2,1)} %k_hbm.1, bf16[128,128]{1,0:T(8,128)(2,1)} %v_hbm.1, f32[4]{0:T(128)} %sink_hbm.1, bf16[256,2048]{1,0:T(8,128)(2,1)} %wo_hbm.1, bf16[32,2048]{1,0:T(8,128)(2,1)} %res_hbm.1, f32[1,2048]{1,0:T(1,128)} %bitcast.3, ...), custom_call_target="tpu_custom_call" | custom-call | tf_op jit(solution)/shard_map/pallas_call | solution.py:961
  42.2 0.7 %copy.17 = bf16[32,2048]{1,0:T(8,128)(2,1)} copy(bf16[32,2048]{1,0:T(8,128)(2,1)S(1)} %shard_map.145) | data formatting | bytes 262144

commit v5 on v4

--- a/solution.py
+++ b/solution.py
@@ -235,15 +235,15 @@
         ("A", 2, "m", 0),
         ("D", (0, 2)),
         ("E", 2),
+        ("E", 0),
         ("G", 3, 1),
         ("Q", 0),
         ("S", "m", 0, 1),
-        ("E", 0),
+        ("F", 0, 0),
+        ("F", 0, 1),
         ("F", 2, 1),
-        ("F", 0, 0),
         ("F", 3, 1),
         ("G", 0, 0),
-        ("F", 0, 1),
         ("S", "m", 3, 0),
         ("F", 2, 0),
         ("G", 0, 1),

time: 43 us -> 42.6 us (level)
    pallas_call x1, Pallas kernels: 42.2 us -> 41.8 us  [fused(): pl.pallas_call(functools.partial(fused_kernel, sp, tp), out_shape=pltpu.V...]
where the time goes in v5:
time: 42.6 us; the launch traced here: 42.5 us
  Pallas kernels  41.8 us (98%)
  local copies, waits for them, and re-layouts  0.66 us (2%)
    pallas_call x1, Pallas kernels, fused(): pl.pallas_call(functools.partial(fused_kernel, sp, tp), out_shape=pltpu.V...  41.8 us

profile of v5, /device:TPU:0, one launch (start us, length us, event | category | flops | bytes accessed | tf_op | source)
XLA Modules:
  0.0 42.5 jit_solution(6413244572958135369)
XLA Ops:
  0.0 41.8 %shard_map.145 = bf16[32,2048]{1,0:T(8,128)(2,1)S(1)} custom-call(bf16[128,256]{1,0:T(8,128)(2,1)} %q_hbm.1, bf16[128,128]{1,0:T(8,128)(2,1)} %k_hbm.1, bf16[128,128]{1,0:T(8,128)(2,1)} %v_hbm.1, f32[4]{0:T(128)} %sink_hbm.1, bf16[256,2048]{1,0:T(8,128)(2,1)} %wo_hbm.1, bf16[32,2048]{1,0:T(8,128)(2,1)} %res_hbm.1, f32[1,2048]{1,0:T(1,128)} %bitcast.3, ...), custom_call_target="tpu_custom_call" | custom-call | tf_op jit(solution)/shard_map/pallas_call | solution.py:961
  41.8 0.7 %copy.17 = bf16[32,2048]{1,0:T(8,128)(2,1)} copy(bf16[32,2048]{1,0:T(8,128)(2,1)S(1)} %shard_map.145) | data formatting | bytes 262144
